TPU v7x, 32 devices: a whole 2x2x4 slice. The times are simulated.
32 devices in a mesh: grp: 2 (over y), sp: 4 (over z), tp: 4 (over x, core).
Axes of the slice: x: 2, y: 2, z: 4, core: 2. Of those that a mesh axis runs over, the one named last changes fastest.
Arguments:
- residual: bfloat16 [2048, 2048], P(('grp', 'sp')), parts along dimension 0, may hold values from -6 to 6
- queries: bfloat16 [2048, 1024], P(('grp', 'sp'), 'tp'), parts along dimension 0, may hold values from -400 to 400
- keys: bfloat16 [2048, 1024], P(('grp', 'sp'), 'tp'), parts along dimension 0, may hold values from -8 to 8
- values: bfloat16 [2048, 1024], P(('grp', 'sp'), 'tp'), parts along dimension 0, may hold values from -6 to 6
- log_gates: float32 [2048, 16], P(('grp', 'sp'), 'tp'), parts along dimension 0, may hold values from -126 to 0, as said below
- w_out: bfloat16 [1024, 2048], P('tp'), may hold values from -0.75 to 0.75
- norm_gain: float32 [2048], replicated, may hold values from 0.1 to 1.9
- w_gate: bfloat16 [2048, 5632], P('sp', 'tp'), may hold values from -0.125 to 0.125
- w_up: bfloat16 [2048, 5632], P('sp', 'tp'), may hold values from -0.125 to 0.125
- w_down: bfloat16 [5632, 2048], P('tp', 'sp'), may hold values from -0.078125 to 0.078125
Outputs:
- output: bfloat16 [2048, 2048], P(('grp', 'sp', 'tp')), parts along dimension 0
There are 2 independent parts, one for each index of `grp`. A program takes and returns all parts, laid end to end along the dimension named above; an argument that names none is the same for every part. Nothing has to cross between parts.
Inputs may be any that keep to these rules, and one draw needn't show every extreme that they name: `log_gates`: never rises along positions.
All inputs are finite; a program needn't handle non-finite values.
Results may differ from a plain program's by a relative error of at most 0.014.
Values may be sent and summed in bfloat16 or wider, within the bound.
A program may use at most 128 MiB of HBM per device.

v0:
```python
import math
import jax
import jax.numpy as jnp
from jax import lax
from jax.sharding import PartitionSpec as P


def normalize(rows_in, gain):
    floats = rows_in.astype(jnp.float32)
    scaled = floats * lax.rsqrt(jnp.mean(floats * floats, axis=-1, keepdims=True) + 1e-06)
    return (scaled * gain).astype(jnp.bfloat16)


def attend(queries, keys, values, log_gates):
    row_count = queries.shape[0]
    head_count = log_gates.shape[1]
    head_width = queries.shape[1] // head_count
    score_scale = head_width ** (-0.5)
    first_row = lax.axis_index("sp") * row_count
    query_heads = queries.reshape(row_count, head_count, head_width)
    query_gates = log_gates.T
    query_positions = first_row + jnp.arange(row_count, dtype=jnp.int32)
    initial = (
        jnp.full((head_count, row_count), -1e30, jnp.float32),
        jnp.zeros((head_count, row_count), jnp.float32),
        jnp.zeros((head_count, row_count, head_width), jnp.float32),
    )
    carried = initial
    key_piece = lax.all_gather(keys.astype(jnp.float32), "sp", axis=0, tiled=True).astype(
        jnp.bfloat16
    )
    value_piece = lax.all_gather(values.astype(jnp.float32), "sp", axis=0, tiled=True).astype(
        jnp.bfloat16
    )
    gate_piece = lax.all_gather(log_gates, "sp", axis=0, tiled=True)
    length = key_piece.shape[0]
    block_rows = math.gcd(length, 2048)
    block_count = length // block_rows
    key_blocks = key_piece.reshape(block_count, block_rows, head_count, head_width)
    value_blocks = value_piece.reshape(block_count, block_rows, head_count, head_width)
    gate_blocks = gate_piece.reshape(block_count, block_rows, head_count)
    offsets = jnp.arange(block_count, dtype=jnp.int32) * block_rows

    def one_block(state, inputs):
        current_key_block, value_block, gate_block, offset = inputs

        def work(current):
            running_max, running_sum, accumulated = current
            scores = (
                jnp.einsum(
                    "qhd,khd->hqk",
                    query_heads,
                    current_key_block,
                    preferred_element_type=jnp.float32,
                )
                * score_scale
            )
            scores = scores + query_gates[:, :, None] - gate_block.T[:, None, :]
            key_positions = offset + jnp.arange(block_rows, dtype=jnp.int32)
            causal = (query_positions[:, None] >= key_positions[None, :])[None]
            scores = jnp.where(causal, scores, -1e30)
            new_max = jnp.maximum(running_max, jnp.max(scores, axis=-1))
            weights = jnp.where(causal, jnp.exp(scores - new_max[:, :, None]), 0.0)
            rescale = jnp.exp(running_max - new_max)
            running_sum = running_sum * rescale + jnp.sum(weights, axis=-1)
            product = jnp.einsum(
                "hqk,khd->hqd",
                weights.astype(jnp.bfloat16),
                value_block,
                preferred_element_type=jnp.float32,
            )
            accumulated = accumulated * rescale[:, :, None] + product
            return (new_max, running_sum, accumulated)

        state = lax.cond(offset <= first_row + row_count - 1, work, lambda current: current, state)
        return (state, None)

    carried, _ = lax.scan(one_block, carried, (key_blocks, value_blocks, gate_blocks, offsets))
    running_max, running_sum, accumulated = carried
    attended = accumulated / running_sum[:, :, None]
    return (
        attended.transpose(1, 0, 2).reshape(row_count, head_count * head_width).astype(jnp.bfloat16)
    )


def body(residual, queries, keys, values, log_gates, w_out, norm_gain, w_gate, w_up, w_down):
    attended = attend(queries, keys, values, log_gates)
    row_count = attended.shape[0]
    per_device = row_count // lax.axis_size("tp")
    my_first = lax.axis_index("tp") * per_device
    projected = lax.psum(
        jnp.dot(attended, w_out, preferred_element_type=jnp.float32).astype(jnp.bfloat16), "tp"
    ).astype(jnp.float32)
    mixed_all = (residual.astype(jnp.float32) + projected).astype(jnp.bfloat16)
    normed_all = normalize(mixed_all, norm_gain)
    mixed = lax.dynamic_slice_in_dim(mixed_all, my_first, per_device, 0)
    gate_whole = lax.all_gather(w_gate, "sp", axis=0, tiled=True)
    up_whole = lax.all_gather(w_up, "sp", axis=0, tiled=True)
    down_whole = lax.all_gather(w_down, "sp", axis=1, tiled=True)
    gate_proj = jnp.dot(normed_all, gate_whole, preferred_element_type=jnp.float32)
    up_proj = jnp.dot(normed_all, up_whole, preferred_element_type=jnp.float32)
    hidden = (jax.nn.silu(gate_proj) * up_proj).astype(jnp.bfloat16)
    down_sum = lax.psum_scatter(
        jnp.dot(hidden, down_whole, preferred_element_type=jnp.float32).astype(jnp.bfloat16),
        "tp",
        scatter_dimension=0,
        tiled=True,
    ).astype(jnp.float32)
    summed = mixed.astype(jnp.float32) + 0.5 * down_sum
    scaled = summed * lax.rsqrt(jnp.mean(summed * summed, axis=-1, keepdims=True) + 1e-06)
    return scaled.astype(jnp.bfloat16)


def solution(mesh):
    in_specs = (
        P(("grp", "sp"), None),
        P(("grp", "sp"), "tp"),
        P(("grp", "sp"), "tp"),
        P(("grp", "sp"), "tp"),
        P(("grp", "sp"), "tp"),
        P("tp", None),
        P(),
        P("sp", "tp"),
        P("sp", "tp"),
        P("tp", "sp"),
    )
    out_specs = P(("grp", "sp", "tp"), None)
    return jax.shard_map(body, mesh=mesh, in_specs=in_specs, out_specs=out_specs, check_vma=False)
```

profile of v0, /device:TPU:0, one launch (start us, length us, event | category | flops | bytes accessed | tf_op | source)
XLA Modules:
  0.0 429.7 jit_solution(2206887288210929115)
XLA Ops:
  7.4 1.1 copy.12
  8.5 17.4 %all_gather.18 = bf16[1024,256]{0,1:T(8,128)(2,1)S(1)} all-gather(bf16[256,256]{0,1:T(8,128)(2,1)S(1)} %copy.12), channel_id=1, replica_groups=mesh['grp'=2,'sp'=4,'tp'=4] {'sp'}, dimensions={0}, use_global_device_ids=true | all-gather | bytes 655360 | tf_op jit(solution)/shard_map/all_gather | solution.py:29
  25.8 1.0 copy.13
  26.9 16.3 %all_gather.20 = bf16[1024,256]{0,1:T(8,128)(2,1)S(1)} all-gather(bf16[256,256]{0,1:T(8,128)(2,1)S(1)} %copy.13), channel_id=1, replica_groups=mesh['grp'=2,'sp'=4,'tp'=4] {'sp'}, dimensions={0}, use_global_device_ids=true | all-gather | bytes 655360 | tf_op jit(solution)/shard_map/all_gather | solution.py:32
  43.1 13.3 %all_gather.19 = f32[1024,4]{0,1:T(4,128)S(1)} all-gather(f32[256,4]{0,1:T(4,128)} %param.16), channel_id=1, replica_groups=mesh['grp'=2,'sp'=4,'tp'=4] {'sp'}, dimensions={0}, use_global_device_ids=true | all-gather | bytes 20480 | tf_op jit(solution)/shard_map/all_gather | solution.py:35
  56.5 7.0 %conditional.1 = ((f32[4,256]{1,0:T(4,128)S(1)}, f32[4,256,64]{1,2,0:T(8,128)S(1)})) conditional(s32[]{:T(128)} %convert_element_type.64, (f32[4,256]{1,0:T(4,128)S(1)}, f32[4,256,64]{1,2,0:T(8,128)S(1)}) %tuple.22, (s32[]{:T(128)}, s32[256]{0:T(256)S(1)}, bf16[256,256]{1,0:T(8,128)(2,1)}, bf16[1024,256]{0,1:T(8,128)(2,1)S(1)}, f32[4,256]{1,0:T(4,128)}, ...), branch_computations={%region_0.1_spmd, %region_1.0_spmd} | conditional | flops 288754944 | bytes 15727672 | solution.py:75
  56.5 0.0 copy-start.2
  56.6 0.2 iota_compare_fusion
  56.8 1.0 copy.14
  57.8 2.1 fusion.2
  59.9 2.0 fusion.1
  61.9 1.6 fusion.6
  63.6 1.4 convolution_convert_fusion
  65.0 0.0 all-reduce.2.cloned.1.call-update
  65.0 0.0 all-gather.4.cloned.1.call-start
  65.1 0.5 all-gather.4.cloned.1.call-update
  65.6 0.0 all-gather.6.cloned.1.call-start
  65.7 0.5 all-gather.6.cloned.1.call-update
  66.2 0.0 all-gather.8.cloned.1.call-start
  66.3 0.5 all-gather.8.cloned.1.call-update
  66.8 0.0 reduce-scatter.2.cloned.1.call-start
  66.8 35.4 %all-reduce.2.cloned.1.call-done = bf16[256,2048]{1,0:T(8,128)(2,1)} async-done(((bf16[256,2048]{1,0:T(8,128)(2,1)}), bf16[256,2048]{1,0:T(8,128)(2,1)}) %all-reduce.2.cloned.1.call-update) | async-done | bytes 1048592 | tf_op jit(solution)/shard_map/psum | solution.py:91
  102.2 1.7 fusion.13
  104.0 70.1 %all-gather.4.cloned.1.call-done = bf16[2048,1408]{1,0:T(8,128)(2,1)} async-done(((bf16[512,1408]{1,0:T(8,128)(2,1)}), bf16[2048,1408]{1,0:T(8,128)(2,1)}) %all-gather.4.cloned.1.call-update) | async-done | bytes 5767184 | tf_op jit(solution)/shard_map/all_gather | solution.py:97
  174.1 5.6 %fusion.18 = f32[256,1408]{1,0:T(8,128)} fusion(bf16[2048,1408]{1,0:T(8,128)(2,1)} %all-gather.4.cloned.1.call-done, bf16[256,2048]{1,0:T(8,128)(2,1)S(1)} %get-tuple-element.132, f32[2048]{0:T(1024)S(1)} %copy-done.3, f32[256]{0:T(256)S(1)} %add_rsqrt_fusion), kind=kOutput, calls=%fused_computation.29 | convolution fusion | flops 1478492160 | bytes 8266752 | tf_op jit(solution)/shard_map/dot_general | solution.py:100
  179.8 100.6 %all-gather.6.cloned.1.call-done = bf16[2048,1408]{1,0:T(8,128)(2,1)} async-done(((bf16[512,1408]{1,0:T(8,128)(2,1)}), bf16[2048,1408]{1,0:T(8,128)(2,1)}) %all-gather.6.cloned.1.call-update) | async-done | bytes 5767184 | tf_op jit(solution)/shard_map/all_gather | solution.py:98
  280.4 106.3 %all-gather.8.cloned.1.call-done = bf16[1408,2048]{1,0:T(8,128)(2,1)} async-done(((bf16[1408,512]{1,0:T(8,128)(2,1)}), bf16[1408,2048]{1,0:T(8,128)(2,1)}) %all-gather.8.cloned.1.call-update) | async-done | bytes 5767184 | tf_op jit(solution)/shard_map/all_gather | solution.py:99
  386.7 9.3 %convolution_convert_fusion.1 = bf16[256,2048]{1,0:T(8,128)(2,1)} fusion(bf16[1408,2048]{1,0:T(8,128)(2,1)} %all-gather.8.cloned.1.call-done, bf16[2048,1408]{1,0:T(8,128)(2,1)} %all-gather.6.cloned.1.call-done, f32[256,1408]{1,0:T(8,128)} %fusion.18, bf16[256,2048]{1,0:T(8,128)(2,1)S(1)} %get-tuple-element.132, f32[2048]{0:T(1024)S(1)} %copy-done.3, ...), kind=kOutput, calls=%fused_computation.21 | convolution fusion | flops 2957574144 | bytes 15082496 | tf_op jit(solution)/shard_map/dot_general | solution.py:104
  395.9 0.0 reduce-scatter.2.cloned.1.call-update
  396.0 23.2 %reduce-scatter.2.cloned.1.call-done = bf16[64,2048]{1,0:T(8,128)(2,1)} async-done(((bf16[256,2048]{1,0:T(8,128)(2,1)}), bf16[64,2048]{1,0:T(8,128)(2,1)}) %reduce-scatter.2.cloned.1.call-update) | async-done | bytes 262160 | tf_op jit(solution)/shard_map/reduce_scatter | solution.py:103
  419.2 1.2 multiply_reduce_fusion
  420.4 1.8 multiply_convert_fusion
  (17 shorter events, 0.1 us)
Async XLA Ops:
  7.4 56.2 %copy-start = (bf16[256,2048]{1,0:T(8,128)(2,1)S(1)}, bf16[256,2048]{1,0:T(8,128)(2,1)}, u32[]{:S(2)}) copy-start(bf16[256,2048]{1,0:T(8,128)(2,1)} %param.17) | copy-start | bytes 3145732
  7.4 94.9 %all-reduce.2.cloned.1.call-start = ((), (), s32[]{:S(2)}) async-start(), calls=%async_computation.1 | async-start | bytes 2097152 | tf_op jit(solution)/shard_map/psum | solution.py:91
  56.5 3.3 copy-start.2
  63.5 38.7 %copy-start.1 = (bf16[256,2048]{1,0:T(8,128)(2,1)S(1)}, bf16[256,2048]{1,0:T(8,128)(2,1)}, u32[]{:S(2)}) copy-start(bf16[256,2048]{1,0:T(8,128)(2,1)} %param.12) | copy-start | bytes 3145732
  65.0 109.1 %copy-start.3 = (f32[2048]{0:T(1024)S(1)}, f32[2048]{0:T(1024)}, u32[]{:S(2)}) copy-start(f32[2048]{0:T(1024)} %param.18) | copy-start | bytes 24580
  65.0 109.1 %all-gather.4.cloned.1.call-start = ((), (), s32[]{:S(2)}) async-start(), calls=%async_computation.2 | async-start | bytes 7208960 | tf_op jit(solution)/shard_map/all_gather | solution.py:97
  65.6 214.8 %all-gather.6.cloned.1.call-start = ((), (), s32[]{:S(2)}) async-start(), calls=%async_computation.3 | async-start | bytes 7208960 | tf_op jit(solution)/shard_map/all_gather | solution.py:98
  66.2 320.5 %all-gather.8.cloned.1.call-start = ((), (), s32[]{:S(2)}) async-start(), calls=%async_computation.4 | async-start | bytes 7208960 | tf_op jit(solution)/shard_map/all_gather | solution.py:99
  66.8 352.4 %reduce-scatter.2.cloned.1.call-start = ((), (), s32[]{:S(2)}) async-start(), calls=%async_computation.5 | async-start | bytes 1310720 | tf_op jit(solution)/shard_map/reduce_scatter | solution.py:103
Sparse Core Ops, SparseCore 0:
  65.2 37.0 all-reduce.1
  396.1 23.0 reduce-scatter.1
Sparse Core Ops, SparseCore 1:
  67.1 107.0 all-gather.3
  175.6 104.8 all-gather.5
  281.9 104.8 all-gather.7
where the time goes:
time: 430 us
  waiting for transfers between devices  337 us (78%)
  blocking collectives  47 us (11%)
  matrix products  20 us (5%)
  between operations  15.1 us (4%)
  other arithmetic  6.94 us (2%)
    all_gather x1, waiting for transfers between devices, body(): down_whole = lax.all_gather(w_down, 'sp', axis=1, tiled=True)  106 us
    all_gather x1, waiting for transfers between devices, body(): up_whole = lax.all_gather(w_up, 'sp', axis=0, tiled=True)  101 us
    all_gather x1, waiting for transfers between devices, body(): gate_whole = lax.all_gather(w_gate, 'sp', axis=0, tiled=True)  70.1 us
    psum x1, waiting for transfers between devices, body(): lax.psum(jnp.dot(attended, w_out, preferred_element_type=jnp.float32).ast...  35.4 us
    reduce_scatter x1, waiting for transfers between devices, body(): lax.psum_scatter(jnp.dot(hidden, down_whole, preferred_element_type=jnp.f...  23.2 us
    all_gather x1, blocking collectives, attend(): lax.all_gather(keys.astype(jnp.float32), 'sp', axis=0, tiled=True)  17.4 us
    all_gather x1, blocking collectives, attend(): lax.all_gather(values.astype(jnp.float32), 'sp', axis=0, tiled=True)  16.3 us
    all_gather x1, blocking collectives, attend(): gate_piece = lax.all_gather(log_gates, 'sp', axis=0, tiled=True)  13.3 us
  transfers between devices with their start and end apart: 5, of which 5 were waited for; matrix products, arithmetic and copies ran while one was open for 2% of the time, Pallas kernels for 0%

commit v1 on v0

--- a/solution.py
+++ b/solution.py
@@ -3,6 +3,17 @@
 import jax.numpy as jnp
 from jax import lax
 from jax.sharding import PartitionSpec as P
+
+
+def pass_along(x, axis, d):
+    count = lax.axis_size(axis)
+    route = [(i, (i + 1) % count) for i in range(count)]
+    blocks = [x]
+    for reach in range(1, count):
+        blocks = [lax.ppermute(blocks[0], axis, route), *blocks]
+    whole = jnp.concatenate(blocks, axis=d)
+    places = (lax.axis_index(axis) + 1) * blocks[-1].shape[d]
+    return jnp.roll(whole, places, axis=d)
 
 
 def normalize(rows_in, gain):
@@ -95,7 +106,7 @@
     normed_all = normalize(mixed_all, norm_gain)
     mixed = lax.dynamic_slice_in_dim(mixed_all, my_first, per_device, 0)
     gate_whole = lax.all_gather(w_gate, "sp", axis=0, tiled=True)
-    up_whole = lax.all_gather(w_up, "sp", axis=0, tiled=True)
+    up_whole = pass_along(w_up, "sp", 0)
     down_whole = lax.all_gather(w_down, "sp", axis=1, tiled=True)
     gate_proj = jnp.dot(normed_all, gate_whole, preferred_element_type=jnp.float32)
     up_proj = jnp.dot(normed_all, up_whole, preferred_element_type=jnp.float32)

time: 430 us -> 386 us (0.90)
  waiting for transfers between devices: 337 us -> 251 us
  starting transfers between devices: 0.17 us -> 27.3 us
  local copies, waits for them, and re-layouts: 3.14 us -> 19.6 us
    ppermute x0 -> x3, waiting for transfers between devices: none -> 151 us  [pass_along(): blocks = [lax.ppermute(blocks[0], axis, route), *blocks]]
    all_gather x1 -> x0, waiting for transfers between devices: 101 us -> none  [body(): up_whole = lax.all_gather(w_up, 'sp', axis=0, tiled=True)]
    all_gather x1, waiting for transfers between devices: 70.1 us -> 0.01 us  [body(): gate_whole = lax.all_gather(w_gate, 'sp', axis=0, tiled=True)]
    psum x1, waiting for transfers between devices: 35.4 us -> 0.01 us  [body(): lax.psum(jnp.dot(attended, w_out, preferred_element_type=jnp.float32).ast...]
    all_gather x1, waiting for transfers between devices: 106 us -> 75 us  [body(): down_whole = lax.all_gather(w_down, 'sp', axis=1, tiled=True)]
    ppermute x0 -> x3, starting transfers between devices: none -> 27.2 us  [pass_along(): blocks = [lax.ppermute(blocks[0], axis, route), *blocks]]
    unnamed x8 -> x19, local copies, waits for them, and re-layouts: 2.1 us -> 17.4 us
  transfers between devices with their start and end apart: 5 -> 7, of which waited for: 5 -> 5; matrix products, arithmetic and copies ran while one was open for 2% -> 6% of each run, Pallas kernels for 0% -> 0%
where the time goes in v1:
time: 386 us; the launch traced here: 385 us
  waiting for transfers between devices  251 us (65%)
  blocking collectives  47 us (12%)
  starting transfers between devices  27.3 us (7%)
  local copies, waits for them, and re-layouts  19.6 us (5%)
  matrix products  18.5 us (5%)
  between operations  15 us (4%)
  other arithmetic  7.37 us (2%)
    ppermute x3, waiting for transfers between devices, pass_along(): blocks = [lax.ppermute(blocks[0], axis, route), *blocks]  151 us
    all_gather x1, waiting for transfers between devices, body(): down_whole = lax.all_gather(w_down, 'sp', axis=1, tiled=True)  75 us
    ppermute x3, starting transfers between devices, pass_along(): blocks = [lax.ppermute(blocks[0], axis, route), *blocks]  27.2 us
    reduce_scatter x1, waiting for transfers between devices, body(): lax.psum_scatter(jnp.dot(hidden, down_whole, preferred_element_type=jnp.f...  23.2 us
    unnamed x19, local copies, waits for them, and re-layouts  17.4 us
    all_gather x1, blocking collectives, attend(): lax.all_gather(keys.astype(jnp.float32), 'sp', axis=0, tiled=True)  17.4 us
    all_gather x1, blocking collectives, attend(): lax.all_gather(values.astype(jnp.float32), 'sp', axis=0, tiled=True)  16.3 us
    all_gather x1, blocking collectives, attend(): gate_piece = lax.all_gather(log_gates, 'sp', axis=0, tiled=True)  13.3 us
  transfers between devices with their start and end apart: 7, of which 5 were waited for; matrix products, arithmetic and copies ran while one was open for 6% of the time, Pallas kernels for 0%

profile of v1, /device:TPU:0, one launch (start us, length us, event | category | flops | bytes accessed | tf_op | source)
XLA Modules:
  0.0 385.5 jit_solution(1594638843056775709)
XLA Ops:
  7.4 1.1 copy.12
  8.5 17.4 %all_gather.15 = bf16[1024,256]{0,1:T(8,128)(2,1)S(1)} all-gather(bf16[256,256]{0,1:T(8,128)(2,1)S(1)} %copy.12), channel_id=1, replica_groups=mesh['grp'=2,'sp'=4,'tp'=4] {'sp'}, dimensions={0}, use_global_device_ids=true | all-gather | bytes 655360 | tf_op jit(solution)/shard_map/all_gather | solution.py:40
  26.9 16.3 %all_gather.17 = bf16[1024,256]{0,1:T(8,128)(2,1)S(1)} all-gather(bf16[256,256]{0,1:T(8,128)(2,1)S(1)} %copy.13), channel_id=1, replica_groups=mesh['grp'=2,'sp'=4,'tp'=4] {'sp'}, dimensions={0}, use_global_device_ids=true | all-gather | bytes 655360 | tf_op jit(solution)/shard_map/all_gather | solution.py:43
  43.1 13.3 %all_gather.16 = f32[1024,4]{0,1:T(4,128)S(1)} all-gather(f32[256,4]{0,1:T(4,128)} %param.16), channel_id=1, replica_groups=mesh['grp'=2,'sp'=4,'tp'=4] {'sp'}, dimensions={0}, use_global_device_ids=true | all-gather | bytes 20480 | tf_op jit(solution)/shard_map/all_gather | solution.py:46
  56.5 7.0 %conditional.1 = ((f32[4,256]{1,0:T(4,128)S(1)}, f32[4,256,64]{1,2,0:T(8,128)S(1)})) conditional(s32[]{:T(128)} %convert_element_type.64, (f32[4,256]{1,0:T(4,128)S(1)}, f32[4,256,64]{1,2,0:T(8,128)S(1)}) %tuple.22, (s32[]{:T(128)}, s32[256]{0:T(256)S(1)}, bf16[256,256]{1,0:T(8,128)(2,1)}, bf16[1024,256]{0,1:T(8,128)(2,1)S(1)}, f32[4,256]{1,0:T(4,128)}, ...), branch_computations={%region_0.1_spmd, %region_1.0_spmd} | conditional | flops 288754944 | bytes 15727672 | solution.py:86
  56.8 1.0 copy.14
  57.8 2.0 fusion.2
  59.9 2.0 fusion.1
  61.9 1.6 fusion.6
  63.6 1.5 convolution_convert_fusion
  66.3 1.0 collective-permute-start
  67.4 53.2 %collective-permute-done = bf16[512,1408]{1,0:T(8,128)(2,1)S(1)} collective-permute-done((bf16[512,1408]{1,0:T(8,128)(2,1)S(1)}, bf16[512,1408]{1,0:T(8,128)(2,1)S(1)}, u32[]{:S(2)}, u32[]{:S(2)}) %collective-permute-start) | collective-permute-done | bytes 1441824 | tf_op jit(solution)/shard_map/ppermute | solution.py:13
  120.6 1.1 copy-done.2
  121.7 13.6 %collective-permute-start.1 = (bf16[512,1408]{1,0:T(8,128)(2,1)S(1)}, bf16[512,1408]{1,0:T(8,128)(2,1)}, u32[]{:S(2)}, u32[]{:S(2)}) collective-permute-start(bf16[512,1408]{1,0:T(8,128)(2,1)S(1)} %collective-permute-done), channel_id=1, source_target_pairs={{0,4},{4,8},{8,12},{12,0},{1,5},{5,9},{9,13},{13,1},{2,6},{6,10},{... | collective-permute-start | bytes 4325384 | tf_op jit(solution)/shard_map/ppermute | solution.py:13
  135.3 67.3 %collective-permute-done.1 = bf16[512,1408]{1,0:T(8,128)(2,1)} collective-permute-done((bf16[512,1408]{1,0:T(8,128)(2,1)S(1)}, bf16[512,1408]{1,0:T(8,128)(2,1)}, u32[]{:S(2)}, u32[]{:S(2)}) %collective-permute-start.1) | collective-permute-done | bytes 1441824 | tf_op jit(solution)/shard_map/ppermute | solution.py:13
  202.6 12.6 %collective-permute-start.2 = (bf16[512,1408]{1,0:T(8,128)(2,1)}, bf16[512,1408]{1,0:T(8,128)(2,1)}, u32[]{:S(2)}, u32[]{:S(2)}) collective-permute-start(bf16[512,1408]{1,0:T(8,128)(2,1)} %collective-permute-done.1), channel_id=1, source_target_pairs={{0,4},{4,8},{8,12},{12,0},{1,5},{5,9},{9,13},{13,1},{2,6},{6,10},{... | collective-permute-start | bytes 4325384 | tf_op jit(solution)/shard_map/ppermute | solution.py:13
  215.2 2.2 fusion.20
  217.3 30.8 %collective-permute-done.2 = bf16[512,1408]{1,0:T(8,128)(2,1)} collective-permute-done((bf16[512,1408]{1,0:T(8,128)(2,1)}, bf16[512,1408]{1,0:T(8,128)(2,1)}, u32[]{:S(2)}, u32[]{:S(2)}) %collective-permute-start.2) | collective-permute-done | bytes 1441824 | tf_op jit(solution)/shard_map/ppermute | solution.py:13
  248.1 2.6 constant_dynamic-update-slice_fusion.7
  250.7 2.6 constant_dynamic-update-slice_fusion.6
  253.3 1.2 constant_dynamic-update-slice_fusion.5
  254.5 1.2 constant_dynamic-update-slice_fusion.4
  255.8 2.6 constant_dynamic-update-slice_fusion.3
  258.4 2.7 constant_dynamic-update-slice_fusion.2
  261.1 1.3 constant_dynamic-update-slice_fusion.1
  262.3 1.2 constant_dynamic-update-slice_fusion
  263.5 4.5 %fusion.28 = f32[256,1408]{1,0:T(8,128)S(1)} fusion(bf16[2048,1408]{1,0:T(8,128)(2,1)} %all-gather.3.cloned.1.call-done, bf16[256,2048]{1,0:T(8,128)(2,1)S(1)} %get-tuple-element.132, f32[2048]{0:T(1024)S(1)} %copy-done.5, f32[256]{0:T(256)S(1)} %add_rsqrt_fusion), kind=kOutput, calls=%fused_computation.32 | convolution fusion | flops 1478492160 | bytes 8266752 | tf_op jit(solution)/shard_map/dot_general | solution.py:111
  268.0 75.0 %all-gather.5.cloned.1.call-done = bf16[1408,2048]{1,0:T(8,128)(2,1)} async-done(((bf16[1408,512]{1,0:T(8,128)(2,1)}), bf16[1408,2048]{1,0:T(8,128)(2,1)}) %all-gather.5.cloned.1.call-update) | async-done | bytes 5767184 | tf_op jit(solution)/shard_map/all_gather | solution.py:110
  343.0 8.9 %convolution_convert_fusion.1 = bf16[256,2048]{1,0:T(8,128)(2,1)} fusion(bf16[1408,2048]{1,0:T(8,128)(2,1)} %all-gather.5.cloned.1.call-done, bf16[4096,1408]{1,0:T(8,128)(2,1)} %constant_dynamic-update-slice_fusion, s32[]{:T(128)S(6)} %select_n.29, f32[256,1408]{1,0:T(8,128)S(1)} %fusion.28, bf16[256,2048]{1,0:T(8,128)(2,1)S(1)} %get-tuple-element.132, ...), kind=kOutput, calls=%fused_computation.23 | convolution fusion | flops 2957574144 | bytes 15082500 | tf_op jit(solution)/shard_map/dot_general | solution.py:115
  351.9 23.2 %reduce-scatter.2.cloned.1.call-done = bf16[64,2048]{1,0:T(8,128)(2,1)} async-done(((bf16[256,2048]{1,0:T(8,128)(2,1)}), bf16[64,2048]{1,0:T(8,128)(2,1)}) %reduce-scatter.2.cloned.1.call-update) | async-done | bytes 262160 | tf_op jit(solution)/shard_map/reduce_scatter | solution.py:114
  375.1 1.2 multiply_reduce_fusion
  376.3 1.8 multiply_convert_fusion
  (32 shorter events, 2.6 us)
Async XLA Ops:
  7.4 56.2 %copy-start = (bf16[256,2048]{1,0:T(8,128)(2,1)S(1)}, bf16[256,2048]{1,0:T(8,128)(2,1)}, u32[]{:S(2)}) copy-start(bf16[256,2048]{1,0:T(8,128)(2,1)} %param.17) | copy-start | bytes 3145732
  7.4 207.8 %all-reduce.2.cloned.1.call-start = ((), (), s32[]{:S(2)}) async-start(), calls=%async_computation.1 | async-start | bytes 2097152 | tf_op jit(solution)/shard_map/psum | solution.py:102
  56.5 3.3 copy-start.4
  63.5 2.8 copy-start.1
  65.1 198.5 %all-gather.3.cloned.1.call-start = ((), (), s32[]{:S(2)}) async-start(), calls=%async_computation.2 | async-start | bytes 7208960 | tf_op jit(solution)/shard_map/all_gather | solution.py:108
  65.7 277.4 %all-gather.5.cloned.1.call-start = ((), (), s32[]{:S(2)}) async-start(), calls=%async_computation.3 | async-start | bytes 7208960 | tf_op jit(solution)/shard_map/all_gather | solution.py:110
  66.2 308.9 %reduce-scatter.2.cloned.1.call-start = ((), (), s32[]{:S(2)}) async-start(), calls=%async_computation.4 | async-start | bytes 1310720 | tf_op jit(solution)/shard_map/reduce_scatter | solution.py:114
  66.3 54.3 %collective-permute-start = (bf16[512,1408]{1,0:T(8,128)(2,1)S(1)}, bf16[512,1408]{1,0:T(8,128)(2,1)S(1)}, u32[]{:S(2)}, u32[]{:S(2)}) collective-permute-start(bf16[512,1408]{1,0:T(8,128)(2,1)S(1)} %copy-done.1), channel_id=1, source_target_pairs={{0,4},{4,8},{8,12},{12,0},{1,5},{5,9},{9,13},{13,1},{2,6},{6,10},{... | collective-permute-start | bytes 4325384 | tf_op jit(solution)/shard_map/ppermute | solution.py:13
  120.6 1.1 copy-start.2
  121.7 80.9 %collective-permute-start.1 = (bf16[512,1408]{1,0:T(8,128)(2,1)S(1)}, bf16[512,1408]{1,0:T(8,128)(2,1)}, u32[]{:S(2)}, u32[]{:S(2)}) collective-permute-start(bf16[512,1408]{1,0:T(8,128)(2,1)S(1)} %collective-permute-done), channel_id=1, source_target_pairs={{0,4},{4,8},{8,12},{12,0},{1,5},{5,9},{9,13},{13,1},{2,6},{6,10},{... | collective-permute-start | bytes 4325384 | tf_op jit(solution)/shard_map/ppermute | solution.py:13
  202.6 45.5 %collective-permute-start.2 = (bf16[512,1408]{1,0:T(8,128)(2,1)}, bf16[512,1408]{1,0:T(8,128)(2,1)}, u32[]{:S(2)}, u32[]{:S(2)}) collective-permute-start(bf16[512,1408]{1,0:T(8,128)(2,1)} %collective-permute-done.1), channel_id=1, source_target_pairs={{0,4},{4,8},{8,12},{12,0},{1,5},{5,9},{9,13},{13,1},{2,6},{6,10},{... | collective-permute-start | bytes 4325384 | tf_op jit(solution)/shard_map/ppermute | solution.py:13
  215.2 38.1 %copy-start.3 = (bf16[512,1408]{1,0:T(8,128)(2,1)S(1)}, bf16[512,1408]{1,0:T(8,128)(2,1)}, u32[]{:S(2)}) copy-start(bf16[512,1408]{1,0:T(8,128)(2,1)} %copy-done.2) | copy-start | bytes 4325380
  258.4 5.2 %copy-start.5 = (f32[2048]{0:T(1024)S(1)}, f32[2048]{0:T(1024)}, u32[]{:S(2)}) copy-start(f32[2048]{0:T(1024)} %param.18) | copy-start | bytes 24580
Sparse Core Ops, SparseCore 0:
  65.2 36.9 all-reduce.1
  352.0 23.0 reduce-scatter.1
Sparse Core Ops, SparseCore 1:
  67.1 167.4 all-gather.2
  236.0 106.9 all-gather.4
